TPU v7x, 32 devices: a whole 2x2x4 slice. The times are simulated.
32 devices in a mesh: ep: 8 (over z, y), tp: 4 (over x, core).
Axes of the slice: x: 2, y: 2, z: 4, core: 2. Of those that a mesh axis runs over, the one named last changes fastest.
Arguments:
- value_in: bfloat16 [4096, 1024], P('ep', 'tp'), may hold values from -6 to 6
- gate_in: bfloat16 [4096, 1024], P('ep', 'tp'), may hold values from -6 to 6
- outer_gate: bfloat16 [4096, 1024], P('ep', 'tp'), may hold values from -6 to 6
- conv_weight: bfloat16 [3, 1024], P(None, 'tp'), may hold values from -3.5 to 3.5
- out_weight: bfloat16 [1024, 2048], P('tp'), may hold values from -0.1875 to 0.1875
- moe_tokens: bfloat16 [4096, 2048], P(('ep', 'tp')), may hold values from -6 to 6
- norm_gain: bfloat16 [2048], replicated, may hold values from 0.099609375 to 1.8984375
- routes: int32 [4096, 2], P(('ep', 'tp')), may hold values from 0 to 7, all different within a row; in each aligned block of 128 rows (0 to 127, 128 to 255, ...) at most 48 rows name the same one
- route_weight: float32 [4096, 2], P(('ep', 'tp')), may hold values from 0.1 to 1
- expert_gate: bfloat16 [8, 2048, 6144], P('ep', None, 'tp'), may hold values from -0.125 to 0.125
- expert_up: bfloat16 [8, 2048, 6144], P('ep', None, 'tp'), may hold values from -0.125 to 0.125
- expert_down: bfloat16 [8, 6144, 2048], P('ep', 'tp'), may hold values from -0.078125 to 0.078125
Outputs:
- mixer_out: bfloat16 [4096, 2048], P(('ep', 'tp'))
- moe_out: bfloat16 [4096, 2048], P(('ep', 'tp'))
Inputs may be any that keep to these rules, and one draw needn't show every extreme that they name: `routes`: each row names 2 different experts. Among the rows of one device no expert is named by more than 48 rows, a bound that some blocks reach.
All inputs are finite; a program needn't handle non-finite values.
Results may differ from a plain program's by a relative error of at most 0.012.
Values may be sent and summed in bfloat16 or wider, within the bound.
A program may use at most 128 MiB of HBM per device.

v0:
```python
import jax
import jax.numpy as jnp
from jax import lax
from jax.sharding import PartitionSpec as P


def extended(x, sides, width):
    for axis, dim in sides:
        size, length = (lax.axis_size(axis), x.shape[dim])
        up = [(i, (i + 1) % size) for i in range(size - 1)]
        down = [(j, i) for i, j in up]
        last = lax.slice_in_dim(x, length - width, length, axis=dim)
        leading = lax.slice_in_dim(x, 0, width, axis=dim)
        before = lax.ppermute(last, axis, up)
        after = lax.ppermute(leading, axis, down)
        x = jnp.concatenate([before, x, after], axis=dim)
    return x


def rounded(values):
    return lax.optimization_barrier(values.astype(jnp.bfloat16)).astype(jnp.float32)


def mixer_half(value_in, gate_in, outer_gate, conv_weight, out_weight):
    product = (value_in.astype(jnp.float32) * gate_in.astype(jnp.float32)).astype(jnp.bfloat16)
    padded = extended(product, (("ep", 0),), 1).astype(jnp.float32)
    taps = conv_weight.astype(jnp.float32)
    convolved = padded[:-2] * taps[0] + padded[1:-1] * taps[1] + padded[2:] * taps[2]
    mixed_rows = (outer_gate.astype(jnp.float32) * convolved).astype(jnp.bfloat16)
    return lax.psum_scatter(
        rounded(jnp.dot(mixed_rows, out_weight, preferred_element_type=jnp.float32)).astype(
            jnp.bfloat16
        ),
        "tp",
        scatter_dimension=0,
        tiled=True,
    )


def expert_half(moe_tokens, norm_gain, routes, route_weight, expert_gate, expert_up, expert_down):
    row_total, top_count = routes.shape
    features = moe_tokens.shape[1]
    local_units = expert_gate.shape[2]
    experts = lax.axis_size("ep")
    capacity = 3 * top_count * row_total // (2 * experts)
    tokens_f32 = moe_tokens.astype(jnp.float32)
    normed = (
        tokens_f32
        * lax.rsqrt(jnp.mean(tokens_f32 * tokens_f32, axis=-1, keepdims=True) + 1e-06)
        * norm_gain.astype(jnp.float32)
    ).astype(jnp.bfloat16)
    flat_ids = routes.reshape(row_total * top_count)
    matches = (flat_ids[:, None] == jnp.arange(experts, dtype=jnp.int32)[None, :]).astype(jnp.int32)
    position = jnp.sum((jnp.cumsum(matches, axis=0) - 1) * matches, axis=1)
    slot_ids = flat_ids * capacity + position
    placement = slot_ids[:, None] == jnp.arange(experts * capacity, dtype=jnp.int32)[None, :]
    placement = (
        placement.reshape(row_total, top_count, experts * capacity).sum(axis=1).astype(jnp.bfloat16)
    )
    outgoing = jnp.einsum("rs,rd->sd", placement, normed, preferred_element_type=jnp.float32)
    outgoing = outgoing.astype(jnp.bfloat16).reshape(experts, capacity, features)
    arrived = lax.all_to_all(outgoing, "ep", split_axis=0, concat_axis=0, tiled=True)
    slot_block = lax.all_gather(arrived[:, None], "tp", axis=1, tiled=True)
    lead = slot_block.shape[:-1]
    flat_rows = slot_block.reshape(-1, features)
    gate_act = jnp.dot(flat_rows, expert_gate[0], preferred_element_type=jnp.float32)
    up_act = jnp.dot(flat_rows, expert_up[0], preferred_element_type=jnp.float32)
    hidden = (jax.nn.silu(gate_act) * up_act).astype(jnp.bfloat16).reshape(lead + (local_units,))
    group_rows = experts * capacity
    group_count = group_rows * lax.axis_size("tp") // group_rows
    selected = hidden
    selected = jnp.swapaxes(selected, 0, 1).reshape(group_count * group_rows, local_units)
    summed_back = lax.psum_scatter(
        rounded(jnp.dot(selected, expert_down[0], preferred_element_type=jnp.float32)).astype(
            jnp.bfloat16
        ),
        "tp",
        scatter_dimension=0,
        tiled=True,
    )
    returned = lax.all_to_all(
        summed_back.reshape(experts, capacity, features),
        "ep",
        split_axis=0,
        concat_axis=0,
        tiled=True,
    )
    picked = returned.reshape(group_rows, features)[slot_ids].reshape(
        row_total, top_count, features
    )
    return jnp.sum(route_weight[..., None] * picked.astype(jnp.float32), axis=1).astype(
        jnp.bfloat16
    )


def body(
    value_in,
    gate_in,
    outer_gate,
    conv_weight,
    out_weight,
    moe_tokens,
    norm_gain,
    routes,
    route_weight,
    expert_gate,
    expert_up,
    expert_down,
):
    mixer_out = mixer_half(value_in, gate_in, outer_gate, conv_weight, out_weight)
    moe_out = expert_half(
        moe_tokens, norm_gain, routes, route_weight, expert_gate, expert_up, expert_down
    )
    return (mixer_out, moe_out)


def solution(mesh):
    placed = (
        P("ep", "tp"),
        P("ep", "tp"),
        P("ep", "tp"),
        P(None, "tp"),
        P("tp", None),
        P(("ep", "tp"), None),
        P(),
        P(("ep", "tp"), None),
        P(("ep", "tp"), None),
        P("ep", None, "tp"),
        P("ep", None, "tp"),
        P("ep", "tp", None),
    )
    return jax.shard_map(
        body,
        mesh=mesh,
        in_specs=placed,
        out_specs=(P(("ep", "tp"), None), P(("ep", "tp"), None)),
        check_vma=False,
    )
```

profile of v0, /device:TPU:0, one launch (start us, length us, event | category | flops | bytes accessed | tf_op | source)
XLA Modules:
  0.0 263.8 jit_solution(1294568977329746764)
XLA Ops:
  7.2 0.9 copy.22
  8.4 0.6 reduce-window.6
  9.0 0.2 slice_reduce_fusion
  9.3 0.1 reduce_sum.41
  9.7 0.7 convert_element_type.78
  10.4 1.2 fusion.5
  11.6 1.7 convolution_convert_fusion.2
  13.3 44.2 %all_to_all.10 = bf16[8,48,2048]{2,1,0:T(8,128)(2,1)} all-to-all(bf16[8,48,2048]{2,1,0:T(8,128)(2,1)S(1)} %bitcast.33), channel_id=1, replica_groups=mesh['ep'=8,'tp'=4] {'ep'}, dimensions={0} | all-to-all | bytes 3145728 | tf_op jit(solution)/shard_map/all_to_all | solution.py:62
  57.6 45.5 %all-gather.3.cloned.1.call-done = bf16[8,192,2048]{2,1,0:T(8,128)(2,1)} async-done(((bf16[8,48,2048]{2,1,0:T(8,128)(2,1)}), bf16[8,192,2048]{2,1,0:T(8,128)(2,1)}) %all-gather.3.cloned.1.call-update) | async-done | bytes 6291472 | tf_op jit(solution)/shard_map/all_gather | solution.py:63
  103.1 16.0 %fusion.3 = f32[1536,1536]{1,0:T(8,128)} fusion(bf16[1536,2048]{1,0:T(8,128)(2,1)} %bitcast.44, bf16[1,2048,1536]{2,1,0:T(8,128)(2,1)} %param.21), kind=kOutput, calls=%fused_computation.6 | convolution fusion | flops 9663676416 | bytes 22020096 | tf_op jit(solution)/shard_map/dot_general | solution.py:66
  119.1 13.8 %fusion = bf16[1536,1536]{1,0:T(8,128)(2,1)S(1)} fusion(bf16[1536,2048]{1,0:T(8,128)(2,1)S(1)} %bitcast.45, f32[1536,1536]{1,0:T(8,128)} %fusion.3, bf16[1,2048,1536]{2,1,0:T(8,128)(2,1)S(1)} %bitcast.43), kind=kOutput, calls=%fused_computation.2 | convolution fusion | flops 9677832192 | bytes 26738688 | tf_op jit(solution)/shard_map/dot_general | solution.py:67
  132.9 0.4 copy.26
  133.3 13.8 %convolution_convert_fusion = bf16[1536,2048]{1,0:T(8,128)(2,1)} fusion(bf16[1536,1536]{1,0:T(8,128)(2,1)S(1)} %bitcast.35, bf16[1,1536,2048]{2,1,0:T(8,128)(2,1)} %param.23), kind=kOutput, calls=%fused_computation.3 | convolution fusion | flops 9666822144 | bytes 17301504 | tf_op jit(solution)/shard_map/dot_general | solution.py:74
  147.2 0.9 copy-done.1
  148.2 3.4 %collective-permute-start = (bf16[1,256]{1,0:T(2,128)(2,1)S(1)}, bf16[1,256]{1,0:T(2,128)(2,1)S(1)}, u32[]{:S(2)}, u32[]{:S(2)}) collective-permute-start(bf16[1,256]{1,0:T(2,128)(2,1)S(1)} %get-tuple-element.2), channel_id=1, source_target_pairs={{0,4},{4,8},{8,12},{12,16},{16,20},{20,24},{24,28},{1,5},{5,9},{9,... | collective-permute-start | bytes 1544 | tf_op jit(solution)/shard_map/ppermute | solution.py:14
  151.6 1.3 collective-permute-start.1
  153.0 4.1 %collective-permute-done.1 = bf16[1,256]{1,0:T(2,128)(2,1)S(1)} collective-permute-done((bf16[1,256]{1,0:T(2,128)(2,1)S(1)}, bf16[1,256]{1,0:T(2,128)(2,1)S(1)}, u32[]{:S(2)}, u32[]{:S(2)}) %collective-permute-start.1) | collective-permute-done | bytes 544 | tf_op jit(solution)/shard_map/ppermute | solution.py:15
  157.2 2.2 convolution_convert_fusion.1
  159.3 46.8 %reduce-scatter.5.cloned.1.call-done = bf16[384,2048]{1,0:T(8,128)(2,1)} async-done(((bf16[1536,2048]{1,0:T(8,128)(2,1)}), bf16[384,2048]{1,0:T(8,128)(2,1)}) %reduce-scatter.5.cloned.1.call-update) | async-done | bytes 1572880 | tf_op jit(solution)/shard_map/reduce_scatter | solution.py:73
  206.2 5.5 %all-to-all-start.1 = ((bf16[8,48,2048]{2,1,0:T(8,128)(2,1)}), bf16[8,48,2048]{2,1,0:T(8,128)(2,1)S(1)}, u32[]{:S(2)}, u32[]{:S(2)}) async-start(bf16[8,48,2048]{2,1,0:T(8,128)(2,1)} %bitcast.36), calls=%async_computation.3 | async-start | bytes 3145728 | tf_op jit(solution)/shard_map/all_to_all | solution.py:81
  212.0 36.6 %all-to-all-done.1 = bf16[8,48,2048]{2,1,0:T(8,128)(2,1)S(1)} async-done(((bf16[8,48,2048]{2,1,0:T(8,128)(2,1)}), bf16[8,48,2048]{2,1,0:T(8,128)(2,1)S(1)}, u32[]{:S(2)}, u32[]{:S(2)}) %all-to-all-start.1) | async-done | bytes 1572896 | tf_op jit(solution)/shard_map/all_to_all | solution.py:81
  248.5 2.3 gather_fusion
  250.9 2.4 reshape.104
  253.3 4.0 %multiply_reduce_fusion = bf16[128,2048]{1,0:T(8,128)(2,1)} fusion(f32[128,2,2048]{2,1,0:T(2,128)S(1)} %reshape.104, f32[128,2]{1,0:T(8,128)S(1)} %copy.21), kind=kLoop, calls=%fused_computation.10 | loop fusion | flops 786432 | bytes 2622464 | tf_op jit(solution)/shard_map/reduce_sum | solution.py:91
  (44 shorter events, 1.3 us)
Async XLA Ops:
  7.2 150.0 %copy-start = (bf16[256,2048]{1,0:T(8,128)(2,1)S(1)}, bf16[256,2048]{1,0:T(8,128)(2,1)}, u32[]{:S(2)}) copy-start(bf16[256,2048]{1,0:T(8,128)(2,1)} %param.16) | copy-start | bytes 3145732
  7.2 95.9 %all-gather.3.cloned.1.call-start = ((), (), s32[]{:S(2)}) async-start(), calls=%async_computation.6 | async-start | bytes 7864320 | tf_op jit(solution)/shard_map/all_gather | solution.py:63
  57.5 61.6 %slice-start = ((s8[6291456]{0:T(1024)(128)(4,1)}), s8[2097152]{0:T(1024)(128)(4,1)S(1)}, s32[]{:S(2)}) async-start(s8[6291456]{0:T(1024)(128)(4,1)} %bitcast.42), calls=%async_computation.7 | async-start | bytes 4194304
  57.6 148.6 %reduce-scatter.5.cloned.1.call-start = ((), (), s32[]{:S(2)}) async-start(), calls=%async_computation.5 | async-start | bytes 7864320 | tf_op jit(solution)/shard_map/reduce_scatter | solution.py:73
  103.1 16.1 %slice-start.1 = ((s8[6291456]{0:T(1024)(128)(4,1)}), s8[4194304]{0:T(1024)(128)(4,1)S(1)}, s32[]{:S(2)}) async-start(s8[6291456]{0:T(1024)(128)(4,1)} %bitcast.42), calls=%async_computation.8 | async-start | bytes 8388608
  103.1 16.1 %copy-start.6 = (bf16[8,192,2048]{2,1,0:T(8,128)(2,1)S(1)}, bf16[8,192,2048]{2,1,0:T(8,128)(2,1)}, u32[]{:S(2)}) copy-start(bf16[8,192,2048]{2,1,0:T(8,128)(2,1)} %all-gather.3.cloned.1.call-done) | copy-start | bytes 18874372
  147.1 0.9 copy-start.1
  147.1 1.0 copy-start.2
  147.1 5.8 %copy-start.4 = (bf16[3,256]{1,0:T(4,128)(2,1)S(1)}, bf16[3,256]{1,0:T(4,128)(2,1)}, u32[]{:S(2)}) copy-start(bf16[3,256]{1,0:T(4,128)(2,1)} %param.15) | copy-start | bytes 4612
  147.1 10.0 %copy-start.3 = (bf16[512,256]{1,0:T(8,128)(2,1)S(1)}, bf16[512,256]{1,0:T(8,128)(2,1)}, u32[]{:S(2)}) copy-start(bf16[512,256]{1,0:T(8,128)(2,1)} %param.14) | copy-start | bytes 786436
  147.2 64.7 %copy-start.5 = (f32[128,2]{0,1:T(2,128)S(1)}, f32[128,2]{0,1:T(2,128)}, u32[]{:S(2)}) copy-start(f32[128,2]{0,1:T(2,128)} %param.20) | copy-start | bytes 3076
  147.2 110.1 %reduce-scatter.3.cloned.1.call-start = ((), (), s32[]{:S(2)}) async-start(), calls=%async_computation.4 | async-start | bytes 2621440 | tf_op jit(solution)/shard_map/reduce_scatter | solution.py:30
  148.2 4.7 %collective-permute-start = (bf16[1,256]{1,0:T(2,128)(2,1)S(1)}, bf16[1,256]{1,0:T(2,128)(2,1)S(1)}, u32[]{:S(2)}, u32[]{:S(2)}) collective-permute-start(bf16[1,256]{1,0:T(2,128)(2,1)S(1)} %get-tuple-element.2), channel_id=1, source_target_pairs={{0,4},{4,8},{8,12},{12,16},{16,20},{20,24},{24,28},{1,5},{5,9},{9,... | collective-permute-start | bytes 1544 | tf_op jit(solution)/shard_map/ppermute | solution.py:14
  151.6 5.5 %collective-permute-start.1 = (bf16[1,256]{1,0:T(2,128)(2,1)S(1)}, bf16[1,256]{1,0:T(2,128)(2,1)S(1)}, u32[]{:S(2)}, u32[]{:S(2)}) collective-permute-start(bf16[1,256]{1,0:T(2,128)(2,1)S(1)} %get-tuple-element.3), channel_id=1, source_target_pairs={{4,0},{8,4},{12,8},{16,12},{20,16},{24,20},{28,24},{5,1},{9,5},{13... | collective-permute-start | bytes 1544 | tf_op jit(solution)/shard_map/ppermute | solution.py:15
  206.2 42.4 %all-to-all-start.1 = ((bf16[8,48,2048]{2,1,0:T(8,128)(2,1)}), bf16[8,48,2048]{2,1,0:T(8,128)(2,1)S(1)}, u32[]{:S(2)}, u32[]{:S(2)}) async-start(bf16[8,48,2048]{2,1,0:T(8,128)(2,1)} %bitcast.36), calls=%async_computation.3 | async-start | bytes 3145728 | tf_op jit(solution)/shard_map/all_to_all | solution.py:81
Sparse Core Ops, SparseCore 0:
  57.7 45.3 all-gather.2
  147.3 58.8 reduce-scatter.4
  209.3 31.1 reduce-scatter.2
where the time goes:
time: 264 us
  waiting for transfers between devices  133 us (50%)
  matrix products  47.5 us (18%)
  blocking collectives  44.2 us (17%)
  between operations  13.9 us (5%)
  starting transfers between devices  10.3 us (4%)
  local copies, waits for them, and re-layouts  7.91 us (3%)
  other arithmetic  6.96 us (3%)
    reduce_scatter x1, waiting for transfers between devices, expert_half(): lax.psum_scatter(rounded(jnp.dot(selected, expert_down[0], preferred_elem...  46.8 us
    all_gather x1, waiting for transfers between devices, expert_half(): slot_block = lax.all_gather(arrived[:, None], 'tp', axis=1, tiled=True)  45.5 us
    all_to_all x1, blocking collectives, expert_half(): lax.all_to_all(outgoing, 'ep', split_axis=0, concat_axis=0, tiled=True)  44.2 us
    all_to_all x1, waiting for transfers between devices, expert_half(): lax.all_to_all(summed_back.reshape(experts, capacity, features), 'ep', sp...  36.6 us
    dot_general x1, matrix products, expert_half(): jnp.dot(flat_rows, expert_gate[0], preferred_element_type=jnp.float32)  16 us
    dot_general x1, matrix products, expert_half(): jnp.dot(selected, expert_down[0], preferred_element_type=jnp.float32)  13.8 us
    dot_general x1, matrix products, expert_half(): jnp.dot(flat_rows, expert_up[0], preferred_element_type=jnp.float32)  13.8 us
    all_to_all x1, starting transfers between devices, expert_half(): lax.all_to_all(summed_back.reshape(experts, capacity, features), 'ep', sp...  5.52 us
  transfers between devices with their start and end apart: 6, of which 4 were waited for; matrix products, arithmetic and copies ran while one was open for 4% of the time, Pallas kernels for 0%

commit v1 on v0

--- a/solution.py
+++ b/solution.py
@@ -60,7 +60,7 @@
     outgoing = jnp.einsum("rs,rd->sd", placement, normed, preferred_element_type=jnp.float32)
     outgoing = outgoing.astype(jnp.bfloat16).reshape(experts, capacity, features)
     arrived = lax.all_to_all(outgoing, "ep", split_axis=0, concat_axis=0, tiled=True)
-    slot_block = lax.all_gather(arrived[:, None], "tp", axis=1, tiled=True)
+    slot_block = jnp.concatenate(lax.all_gather(arrived[:, None], "tp"), axis=1)
     lead = slot_block.shape[:-1]
     flat_rows = slot_block.reshape(-1, features)
     gate_act = jnp.dot(flat_rows, expert_gate[0], preferred_element_type=jnp.float32)

time: 264 us -> 266 us (level)
  local copies, waits for them, and re-layouts: 7.91 us -> 11.8 us
    reshape x0 -> x1, local copies, waits for them, and re-layouts: none -> 3.53 us  [expert_half(): slot_block = jnp.concatenate(lax.all_gather(arrived[:, None], 'tp'), axis=1)]
    dot_general x1, matrix products: 16 us -> 12.6 us  [expert_half(): jnp.dot(flat_rows, expert_gate[0], preferred_element_type=jnp.float32)]
where the time goes in v1:
time: 266 us
  waiting for transfers between devices  133 us (50%)
  matrix products  45.3 us (17%)
  blocking collectives  44.2 us (17%)
  between operations  14 us (5%)
  local copies, waits for them, and re-layouts  11.8 us (4%)
  starting transfers between devices  10.3 us (4%)
  other arithmetic  6.96 us (3%)
    reduce_scatter x1, waiting for transfers between devices, expert_half(): lax.psum_scatter(rounded(jnp.dot(selected, expert_down[0], preferred_elem...  46.8 us
    all_gather x1, waiting for transfers between devices, expert_half(): slot_block = jnp.concatenate(lax.all_gather(arrived[:, None], 'tp'), axis=1)  45.5 us
    all_to_all x1, blocking collectives, expert_half(): lax.all_to_all(outgoing, 'ep', split_axis=0, concat_axis=0, tiled=True)  44.2 us
    all_to_all x1, waiting for transfers between devices, expert_half(): lax.all_to_all(summed_back.reshape(experts, capacity, features), 'ep', sp...  36.6 us
    dot_general x1, matrix products, expert_half(): jnp.dot(flat_rows, expert_up[0], preferred_element_type=jnp.float32)  14.8 us
    dot_general x1, matrix products, expert_half(): jnp.dot(selected, expert_down[0], preferred_element_type=jnp.float32)  14 us
    dot_general x1, matrix products, expert_half(): jnp.dot(flat_rows, expert_gate[0], preferred_element_type=jnp.float32)  12.6 us
    all_to_all x1, starting transfers between devices, expert_half(): lax.all_to_all(summed_back.reshape(experts, capacity, features), 'ep', sp...  5.52 us
  transfers between devices with their start and end apart: 6, of which 4 were waited for; matrix products, arithmetic and copies ran while one was open for 4% of the time, Pallas kernels for 0%

profile of v1, /device:TPU:0, one launch (start us, length us, event | category | flops | bytes accessed | tf_op | source)
XLA Modules:
  0.0 265.5 jit_solution(10810887587579361720)
XLA Ops:
  7.2 0.9 copy.34
  8.4 0.6 reduce-window.6
  9.7 0.7 convert_element_type.78
  10.4 1.2 fusion.5
  11.6 1.7 convolution_convert_fusion.2
  13.3 44.2 %all_to_all.10 = bf16[8,48,2048]{2,1,0:T(8,128)(2,1)} all-to-all(bf16[8,48,2048]{2,1,0:T(8,128)(2,1)S(1)} %bitcast.39), channel_id=1, replica_groups=mesh['ep'=8,'tp'=4] {'ep'}, dimensions={0} | all-to-all | bytes 3145728 | tf_op jit(solution)/shard_map/all_to_all | solution.py:62
  57.6 45.5 %all-gather.3.cloned.1.call-done = bf16[32,48,2048]{2,1,0:T(8,128)(2,1)} async-done(((bf16[8,48,2048]{2,1,0:T(8,128)(2,1)}), bf16[32,48,2048]{2,1,0:T(8,128)(2,1)}) %all-gather.3.cloned.1.call-update) | async-done | bytes 6291472 | tf_op jit(solution)/shard_map/all_gather | solution.py:63
  103.1 3.5 %copy.38 = bf16[8,4,1,48,2048]{4,3,1,0,2:T(8,128)(2,1)S(1)} copy(bf16[8,4,1,48,2048]{4,3,0,1,2:T(8,128)(2,1)} %bitcast.36) | data formatting | bytes 12582912 | tf_op jit(solution)/shard_map/reshape | solution.py:63
  106.6 0.5 slice-done.1
  107.1 12.6 %fusion.3 = f32[1536,1536]{1,0:T(8,128)} fusion(bf16[1536,2048]{1,0:T(8,128)(2,1)S(1)} %bitcast.37, bf16[1,2048,1536]{2,1,0:T(8,128)(2,1)S(1)} %bitcast.49), kind=kOutput, calls=%fused_computation.6 | convolution fusion | flops 9663676416 | bytes 22020096 | tf_op jit(solution)/shard_map/dot_general | solution.py:66
  119.7 14.8 %fusion = bf16[1536,1536]{1,0:T(8,128)(2,1)S(1)} fusion(bf16[1536,2048]{1,0:T(8,128)(2,1)S(1)} %bitcast.38, f32[1536,1536]{1,0:T(8,128)} %fusion.3, bf16[1,2048,1536]{2,1,0:T(8,128)(2,1)} %param.22), kind=kOutput, calls=%fused_computation.2 | convolution fusion | flops 9677832192 | bytes 26738688 | tf_op jit(solution)/shard_map/dot_general | solution.py:67
  134.5 0.3 copy.39
  134.8 14.0 %convolution_convert_fusion = bf16[1536,2048]{1,0:T(8,128)(2,1)} fusion(bf16[1536,1536]{1,0:T(8,128)(2,1)S(1)} %bitcast.41, bf16[1,1536,2048]{2,1,0:T(8,128)(2,1)} %param.23), kind=kOutput, calls=%fused_computation.3 | convolution fusion | flops 9666822144 | bytes 17301504 | tf_op jit(solution)/shard_map/dot_general | solution.py:74
  148.9 0.9 copy-done.1
  149.9 3.4 %collective-permute-start = (bf16[1,256]{1,0:T(2,128)(2,1)S(1)}, bf16[1,256]{1,0:T(2,128)(2,1)S(1)}, u32[]{:S(2)}, u32[]{:S(2)}) collective-permute-start(bf16[1,256]{1,0:T(2,128)(2,1)S(1)} %get-tuple-element.2), channel_id=1, source_target_pairs={{0,4},{4,8},{8,12},{12,16},{16,20},{20,24},{24,28},{1,5},{5,9},{9,... | collective-permute-start | bytes 1544 | tf_op jit(solution)/shard_map/ppermute | solution.py:14
  153.3 1.3 collective-permute-start.1
  154.6 4.1 %collective-permute-done.1 = bf16[1,256]{1,0:T(2,128)(2,1)S(1)} collective-permute-done((bf16[1,256]{1,0:T(2,128)(2,1)S(1)}, bf16[1,256]{1,0:T(2,128)(2,1)S(1)}, u32[]{:S(2)}, u32[]{:S(2)}) %collective-permute-start.1) | collective-permute-done | bytes 544 | tf_op jit(solution)/shard_map/ppermute | solution.py:15
  158.8 2.2 convolution_convert_fusion.1
  161.0 46.8 %reduce-scatter.5.cloned.1.call-done = bf16[384,2048]{1,0:T(8,128)(2,1)} async-done(((bf16[1536,2048]{1,0:T(8,128)(2,1)}), bf16[384,2048]{1,0:T(8,128)(2,1)}) %reduce-scatter.5.cloned.1.call-update) | async-done | bytes 1572880 | tf_op jit(solution)/shard_map/reduce_scatter | solution.py:73
  207.9 5.5 %all-to-all-start.1 = ((bf16[8,48,2048]{2,1,0:T(8,128)(2,1)}), bf16[8,48,2048]{2,1,0:T(8,128)(2,1)S(1)}, u32[]{:S(2)}, u32[]{:S(2)}) async-start(bf16[8,48,2048]{2,1,0:T(8,128)(2,1)} %bitcast.42), calls=%async_computation.3 | async-start | bytes 3145728 | tf_op jit(solution)/shard_map/all_to_all | solution.py:81
  213.7 36.6 %all-to-all-done.1 = bf16[8,48,2048]{2,1,0:T(8,128)(2,1)S(1)} async-done(((bf16[8,48,2048]{2,1,0:T(8,128)(2,1)}), bf16[8,48,2048]{2,1,0:T(8,128)(2,1)S(1)}, u32[]{:S(2)}, u32[]{:S(2)}) %all-to-all-start.1) | async-done | bytes 1572896 | tf_op jit(solution)/shard_map/all_to_all | solution.py:81
  250.2 2.3 gather_fusion
  252.6 2.4 reshape.104
  254.9 4.0 %multiply_reduce_fusion = bf16[128,2048]{1,0:T(8,128)(2,1)} fusion(f32[128,2,2048]{2,1,0:T(2,128)S(1)} %reshape.104, f32[128,2]{1,0:T(8,128)S(1)} %copy.33), kind=kLoop, calls=%fused_computation.10 | loop fusion | flops 786432 | bytes 2622464 | tf_op jit(solution)/shard_map/reduce_sum | solution.py:91
  (43 shorter events, 1.7 us)
Async XLA Ops:
  7.2 151.7 %copy-start = (bf16[256,2048]{1,0:T(8,128)(2,1)S(1)}, bf16[256,2048]{1,0:T(8,128)(2,1)}, u32[]{:S(2)}) copy-start(bf16[256,2048]{1,0:T(8,128)(2,1)} %param.16) | copy-start | bytes 3145732
  7.2 95.9 %all-gather.3.cloned.1.call-start = ((), (), s32[]{:S(2)}) async-start(), calls=%async_computation.6 | async-start | bytes 7864320 | tf_op jit(solution)/shard_map/all_gather | solution.py:63
  57.5 49.1 %slice-start = ((s8[6291456]{0:T(1024)(128)(4,1)}), s8[2097152]{0:T(1024)(128)(4,1)S(1)}, s32[]{:S(2)}) async-start(s8[6291456]{0:T(1024)(128)(4,1)} %bitcast.48), calls=%async_computation.7 | async-start | bytes 4194304
  57.6 150.3 %reduce-scatter.5.cloned.1.call-start = ((), (), s32[]{:S(2)}) async-start(), calls=%async_computation.5 | async-start | bytes 7864320 | tf_op jit(solution)/shard_map/reduce_scatter | solution.py:73
  103.1 4.0 %slice-start.1 = ((s8[6291456]{0:T(1024)(128)(4,1)}), s8[4194304]{0:T(1024)(128)(4,1)S(1)}, s32[]{:S(2)}) async-start(s8[6291456]{0:T(1024)(128)(4,1)} %bitcast.48), calls=%async_computation.8 | async-start | bytes 8388608
  148.8 0.9 copy-start.1
  148.8 1.0 copy-start.2
  148.8 5.8 %copy-start.4 = (bf16[3,256]{1,0:T(4,128)(2,1)S(1)}, bf16[3,256]{1,0:T(4,128)(2,1)}, u32[]{:S(2)}) copy-start(bf16[3,256]{1,0:T(4,128)(2,1)} %param.15) | copy-start | bytes 4612
  148.8 10.0 %copy-start.3 = (bf16[512,256]{1,0:T(8,128)(2,1)S(1)}, bf16[512,256]{1,0:T(8,128)(2,1)}, u32[]{:S(2)}) copy-start(bf16[512,256]{1,0:T(8,128)(2,1)} %param.14) | copy-start | bytes 786436
  148.8 64.7 %copy-start.5 = (f32[128,2]{0,1:T(2,128)S(1)}, f32[128,2]{0,1:T(2,128)}, u32[]{:S(2)}) copy-start(f32[128,2]{0,1:T(2,128)} %param.20) | copy-start | bytes 3076
  148.8 110.1 %reduce-scatter.3.cloned.1.call-start = ((), (), s32[]{:S(2)}) async-start(), calls=%async_computation.4 | async-start | bytes 2621440 | tf_op jit(solution)/shard_map/reduce_scatter | solution.py:30
  149.9 4.7 %collective-permute-start = (bf16[1,256]{1,0:T(2,128)(2,1)S(1)}, bf16[1,256]{1,0:T(2,128)(2,1)S(1)}, u32[]{:S(2)}, u32[]{:S(2)}) collective-permute-start(bf16[1,256]{1,0:T(2,128)(2,1)S(1)} %get-tuple-element.2), channel_id=1, source_target_pairs={{0,4},{4,8},{8,12},{12,16},{16,20},{20,24},{24,28},{1,5},{5,9},{9,... | collective-permute-start | bytes 1544 | tf_op jit(solution)/shard_map/ppermute | solution.py:14
  153.3 5.5 %collective-permute-start.1 = (bf16[1,256]{1,0:T(2,128)(2,1)S(1)}, bf16[1,256]{1,0:T(2,128)(2,1)S(1)}, u32[]{:S(2)}, u32[]{:S(2)}) collective-permute-start(bf16[1,256]{1,0:T(2,128)(2,1)S(1)} %get-tuple-element.3), channel_id=1, source_target_pairs={{4,0},{8,4},{12,8},{16,12},{20,16},{24,20},{28,24},{5,1},{9,5},{13... | collective-permute-start | bytes 1544 | tf_op jit(solution)/shard_map/ppermute | solution.py:15
  207.9 42.4 %all-to-all-start.1 = ((bf16[8,48,2048]{2,1,0:T(8,128)(2,1)}), bf16[8,48,2048]{2,1,0:T(8,128)(2,1)S(1)}, u32[]{:S(2)}, u32[]{:S(2)}) async-start(bf16[8,48,2048]{2,1,0:T(8,128)(2,1)} %bitcast.42), calls=%async_computation.3 | async-start | bytes 3145728 | tf_op jit(solution)/shard_map/all_to_all | solution.py:81
Sparse Core Ops, SparseCore 0:
  57.7 45.3 all-gather.2
  149.0 58.8 reduce-scatter.4
  211.0 31.1 reduce-scatter.2
